TPU v7x, 32 devices: a whole 2x2x4 slice. The times are simulated.
32 devices in a mesh: rep: 8 (over z, y), fs: 2 (over x), tp: 2 (over core).
Axes of the slice: x: 2, y: 2, z: 4, core: 2. Of those that a mesh axis runs over, the one named last changes fastest.
Arguments:
- inputs: bfloat16 [4096, 2048], P(('rep', 'tp'), 'fs'), may hold values from -6 to 6
- pre_act: bfloat16 [4096, 4096], P(('rep', 'fs'), 'tp'), may hold values from -6 to 6
- cotangent: bfloat16 [4096, 2048], P(('rep', 'tp'), 'fs'), may hold values from -6 to 6
- up_weight: bfloat16 [2048, 4096], P('fs', 'tp'), may hold values from -0.125 to 0.125
- down_weight: bfloat16 [4096, 2048], P('tp', 'fs'), may hold values from -0.09375 to 0.09375
Outputs:
- grad_inputs: bfloat16 [4096, 2048], P(('rep', 'tp'), 'fs')
- grad_up: float32 [2048, 4096], P('fs', 'tp')
- grad_down: float32 [4096, 2048], P('tp', 'fs')
All inputs are finite; a program needn't handle non-finite values.
Results may differ from a plain program's by a relative error of at most 0.015.
Values may be sent and summed in bfloat16 or wider, within the bound.
A program may use at most 128 MiB of HBM per device.

v0:
```python
import jax
import jax.numpy as jnp
from jax import lax
from jax.sharding import PartitionSpec as P


def contract_rows(left, right):
    return lax.dot_general(
        left, right, (((0,), (0,)), ((), ())), preferred_element_type=jnp.float32
    )


def contract_cols(left, right):
    return lax.dot_general(
        left, right, (((1,), (1,)), ((), ())), preferred_element_type=jnp.float32
    )


def per_device(inputs, pre_act, cotangent, up_weight, down_weight):
    group_x, group_cot = (
        lax.all_gather(inputs, "tp", axis=0, tiled=True),
        lax.all_gather(cotangent, "tp", axis=0, tiled=True),
    )
    positive = jnp.maximum(pre_act.astype(jnp.float32), 0.0)
    square = (positive * positive).astype(jnp.bfloat16)
    rows_block = group_cot
    grad_act = lax.psum_scatter(
        contract_cols(rows_block, down_weight).astype(jnp.bfloat16),
        "fs",
        scatter_dimension=0,
        tiled=True,
    ).astype(jnp.float32)
    grad_pre = (2.0 * positive * grad_act).astype(jnp.bfloat16)
    factor = (inputs.shape[0] * lax.axis_size("rep") * lax.axis_size("tp")) ** (-0.5)
    group_grad, group_square = (
        lax.all_gather(grad_pre, "fs", axis=0, tiled=True),
        lax.all_gather(square, "fs", axis=0, tiled=True),
    )
    down_part = contract_rows(group_square, group_cot)
    up_part = contract_rows(group_x, group_grad)
    up_slice, down_slice = (
        lax.psum_scatter(up_part, "rep", scatter_dimension=0, tiled=True),
        lax.psum_scatter(down_part, "rep", scatter_dimension=0, tiled=True),
    )
    grad_up, grad_down = (
        lax.all_gather(up_slice.astype(jnp.bfloat16), "rep", axis=0, tiled=True).astype(
            up_slice.dtype
        ),
        lax.all_gather(down_slice.astype(jnp.bfloat16), "rep", axis=0, tiled=True).astype(
            down_slice.dtype
        ),
    )
    rows_block = group_grad
    grad_inputs = lax.psum_scatter(
        contract_cols(rows_block, up_weight).astype(jnp.bfloat16),
        "tp",
        scatter_dimension=0,
        tiled=True,
    )
    return (grad_inputs, grad_up * factor, grad_down * factor)


def solution(mesh):
    placed = (
        P(("rep", "tp"), "fs"),
        P(("rep", "fs"), "tp"),
        P(("rep", "tp"), "fs"),
        P("fs", "tp"),
        P("tp", "fs"),
    )
    return jax.shard_map(
        per_device,
        mesh=mesh,
        in_specs=placed,
        out_specs=(P(("rep", "tp"), "fs"), P("fs", "tp"), P("tp", "fs")),
        check_vma=False,
    )
```

profile of v0, /device:TPU:0, one launch (start us, length us, event | category | flops | bytes accessed | tf_op | source)
XLA Modules:
  0.0 611.5 jit_solution(11408372984345961125)
XLA Ops:
  7.2 0.0 all-gather.7.cloned.1.call-start
  7.2 0.7 all-gather.7.cloned.1.call-update
  7.9 0.0 copy-start
  7.9 0.0 reduce-scatter.5.cloned.1.call-start
  8.0 13.3 %all-gather.7.cloned.1.call-done = bf16[512,1024]{1,0:T(8,128)(2,1)} async-done(((bf16[256,1024]{1,0:T(8,128)(2,1)}), bf16[512,1024]{1,0:T(8,128)(2,1)}) %all-gather.7.cloned.1.call-update) | async-done | bytes 1048592 | tf_op jit(solution)/shard_map/all_gather | solution.py:22
  21.3 6.2 %convolution_convert_fusion = bf16[512,2048]{1,0:T(8,128)(2,1)} fusion(bf16[512,1024]{1,0:T(8,128)(2,1)} %all-gather.7.cloned.1.call-done, bf16[2048,1024]{1,0:T(8,128)(2,1)} %param.9), kind=kOutput, calls=%fused_computation.3 | convolution fusion | flops 2148532224 | bytes 7340032 | tf_op jit(solution)/shard_map/dot_general | solution.py:14
  27.5 0.0 reduce-scatter.5.cloned.1.call-update
  27.5 0.0 all-gather.11.cloned.1.call-start
  27.6 0.7 all-gather.11.cloned.1.call-update
  28.3 0.0 all-gather.9.cloned.1.call-start
  28.3 32.5 %reduce-scatter.5.cloned.1.call-done = bf16[256,2048]{1,0:T(8,128)(2,1)} async-done(((bf16[512,2048]{1,0:T(8,128)(2,1)}), bf16[256,2048]{1,0:T(8,128)(2,1)}) %reduce-scatter.5.cloned.1.call-update) | async-done | bytes 1048592 | tf_op jit(solution)/shard_map/reduce_scatter | solution.py:27
  60.8 0.0 copy-done
  60.8 3.1 multiply_convert_fusion
  63.9 0.0 all-gather.9.cloned.1.call-update
  63.9 0.0 all-gather.15.cloned.1.call-start
  64.0 0.5 all-gather.15.cloned.1.call-update
  64.5 0.0 reduce-scatter.9.cloned.1.call-start
  64.5 6.8 %all-gather.11.cloned.1.call-done = bf16[512,1024]{1,0:T(8,128)(2,1)} async-done(((bf16[256,1024]{1,0:T(8,128)(2,1)}), bf16[512,1024]{1,0:T(8,128)(2,1)}) %all-gather.11.cloned.1.call-update) | async-done | bytes 1048592 | tf_op jit(solution)/shard_map/all_gather | solution.py:21
  71.4 36.3 %all-gather.9.cloned.1.call-done = bf16[512,2048]{1,0:T(8,128)(2,1)} async-done(((bf16[256,2048]{1,0:T(8,128)(2,1)}), bf16[512,2048]{1,0:T(8,128)(2,1)}) %all-gather.9.cloned.1.call-update) | async-done | bytes 2097168 | tf_op jit(solution)/shard_map/all_gather | solution.py:36
  107.7 7.6 %convolution_bitcast_fusion = f32[1024,2048]{0,1:T(8,128)} fusion(bf16[512,2048]{1,0:T(8,128)(2,1)} %all-gather.9.cloned.1.call-done, bf16[512,1024]{1,0:T(8,128)(2,1)} %all-gather.11.cloned.1.call-done), kind=kOutput, calls=%fused_computation.2 | convolution fusion | flops 2147483648 | bytes 11534336 | tf_op jit(solution)/shard_map/dot_general | solution.py:8
  115.3 0.0 copy-start.2
  115.3 0.0 reduce-scatter.9.cloned.1.call-update
  115.3 0.0 reduce-scatter.11.cloned.1.call-start
  115.4 27.4 %all-gather.15.cloned.1.call-done = bf16[512,2048]{1,0:T(8,128)(2,1)} async-done(((bf16[256,2048]{1,0:T(8,128)(2,1)}), bf16[512,2048]{1,0:T(8,128)(2,1)}) %all-gather.15.cloned.1.call-update) | async-done | bytes 2097168 | tf_op jit(solution)/shard_map/all_gather | solution.py:37
  142.7 0.0 copy-done.2
  142.7 7.4 %fusion = f32[2048,1024]{1,0:T(8,128)} fusion(bf16[512,2048]{1,0:T(8,128)(2,1)} %all-gather.15.cloned.1.call-done, bf16[512,1024]{1,0:T(8,128)(2,1)S(1)} %copy-done.2), kind=kOutput, calls=%fused_computation.8 | convolution fusion | flops 2147483648 | bytes 11534336 | tf_op jit(solution)/shard_map/dot_general | solution.py:8
  150.1 0.0 reduce-scatter.11.cloned.1.call-update
  150.1 0.0 copy-start.1
  150.1 0.0 all-gather.13.cloned.1.call-start
  150.2 144.5 %reduce-scatter.9.cloned.1.call-done = f32[128,2048]{0,1:T(8,128)} async-done(((f32[1024,2048]{0,1:T(8,128)}), f32[128,2048]{0,1:T(8,128)}) %reduce-scatter.9.cloned.1.call-update) | async-done | bytes 1048592 | tf_op jit(solution)/shard_map/reduce_scatter | solution.py:42
  294.7 2.1 convert_element_type.35
  296.8 0.0 all-gather.13.cloned.1.call-update
  296.8 0.0 all-gather.17.cloned.1.call-start
  296.8 148.7 %reduce-scatter.11.cloned.1.call-done = f32[256,1024]{1,0:T(8,128)} async-done(((f32[2048,1024]{1,0:T(8,128)}), f32[256,1024]{1,0:T(8,128)}) %reduce-scatter.11.cloned.1.call-update) | async-done | bytes 1048592 | tf_op jit(solution)/shard_map/reduce_scatter | solution.py:43
  445.5 2.1 convert_element_type.38
  447.6 0.0 all-gather.17.cloned.1.call-update
  447.6 0.2 reduce-scatter.7.cloned.1.call-start
  447.9 0.0 copy-done.1
  447.9 5.6 convolution_convert_fusion.1
  453.5 0.0 reduce-scatter.7.cloned.1.call-update
  453.5 68.4 %all-gather.13.cloned.1.call-done = bf16[1024,2048]{0,1:T(8,128)(2,1)} async-done(((bf16[128,2048]{0,1:T(8,128)(2,1)}), bf16[1024,2048]{0,1:T(8,128)(2,1)}) %all-gather.13.cloned.1.call-update) | async-done | bytes 4194320 | tf_op jit(solution)/shard_map/all_gather | solution.py:46
  521.9 6.8 %convert_multiply_fusion.1 = f32[1024,2048]{0,1:T(8,128)} fusion(bf16[1024,2048]{0,1:T(8,128)(2,1)} %all-gather.13.cloned.1.call-done), kind=kLoop, calls=%fused_computation.1 | loop fusion | flops 4194304 | bytes 12582912 | tf_op jit(solution)/shard_map/mul | solution.py:60
  528.7 9.3 %copy.8 = f32[1024,2048]{1,0:T(8,128)} copy(f32[1024,2048]{0,1:T(8,128)} %convert_multiply_fusion.1) | data formatting | bytes 16777216
  538.0 57.1 %all-gather.17.cloned.1.call-done = bf16[2048,1024]{1,0:T(8,128)(2,1)} async-done(((bf16[256,1024]{1,0:T(8,128)(2,1)}), bf16[2048,1024]{1,0:T(8,128)(2,1)}) %all-gather.17.cloned.1.call-update) | async-done | bytes 4194320 | tf_op jit(solution)/shard_map/all_gather | solution.py:49
  595.0 6.8 %convert_multiply_fusion = f32[2048,1024]{1,0:T(8,128)} fusion(bf16[2048,1024]{1,0:T(8,128)(2,1)} %all-gather.17.cloned.1.call-done), kind=kLoop, calls=%fused_computation | loop fusion | flops 4194304 | bytes 12582912 | tf_op jit(solution)/shard_map/mul | solution.py:60
  601.8 2.8 reduce-scatter.7.cloned.1.call-done
Async XLA Ops:
  7.2 14.1 %all-gather.7.cloned.1.call-start = ((), (), s32[]{:S(2)}) async-start(), calls=%async_computation.4 | async-start | bytes 1572864 | tf_op jit(solution)/shard_map/all_gather | solution.py:22
  7.9 52.9 %copy-start = (bf16[256,2048]{1,0:T(8,128)(2,1)S(1)}, bf16[256,2048]{1,0:T(8,128)(2,1)}, u32[]{:S(2)}) copy-start(bf16[256,2048]{1,0:T(8,128)(2,1)} %param.6) | copy-start | bytes 3145732
  7.9 52.9 %reduce-scatter.5.cloned.1.call-start = ((), (), s32[]{:S(2)}) async-start(), calls=%async_computation.5 | async-start | bytes 3145728 | tf_op jit(solution)/shard_map/reduce_scatter | solution.py:27
  27.5 43.9 %all-gather.11.cloned.1.call-start = ((), (), s32[]{:S(2)}) async-start(), calls=%async_computation.8 | async-start | bytes 1572864 | tf_op jit(solution)/shard_map/all_gather | solution.py:21
  28.3 79.4 %all-gather.9.cloned.1.call-start = ((), (), s32[]{:S(2)}) async-start(), calls=%async_computation.6 | async-start | bytes 3145728 | tf_op jit(solution)/shard_map/all_gather | solution.py:36
  63.9 78.8 %all-gather.15.cloned.1.call-start = ((), (), s32[]{:S(2)}) async-start(), calls=%async_computation.11 | async-start | bytes 3145728 | tf_op jit(solution)/shard_map/all_gather | solution.py:37
  64.5 230.2 %reduce-scatter.9.cloned.1.call-start = ((), (), s32[]{:S(2)}) async-start(), calls=%async_computation.9 | async-start | bytes 9437184 | tf_op jit(solution)/shard_map/reduce_scatter | solution.py:42
  115.3 27.5 %copy-start.2 = (bf16[512,1024]{1,0:T(8,128)(2,1)S(1)}, bf16[512,1024]{1,0:T(8,128)(2,1)}, u32[]{:S(2)}) copy-start(bf16[512,1024]{1,0:T(8,128)(2,1)} %all-gather.7.cloned.1.call-done) | copy-start | bytes 3145732
  115.3 330.2 %reduce-scatter.11.cloned.1.call-start = ((), (), s32[]{:S(2)}) async-start(), calls=%async_computation.12 | async-start | bytes 9437184 | tf_op jit(solution)/shard_map/reduce_scatter | solution.py:43
  150.1 297.7 %copy-start.1 = (bf16[512,2048]{1,0:T(8,128)(2,1)S(1)}, bf16[512,2048]{1,0:T(8,128)(2,1)}, u32[]{:S(2)}) copy-start(bf16[512,2048]{1,0:T(8,128)(2,1)} %all-gather.9.cloned.1.call-done) | copy-start | bytes 6291460
  150.1 371.7 %all-gather.13.cloned.1.call-start = ((), (), s32[]{:S(2)}) async-start(), calls=%async_computation.10 | async-start | bytes 4718592 | tf_op jit(solution)/shard_map/all_gather | solution.py:46
  296.8 298.2 %all-gather.17.cloned.1.call-start = ((), (), s32[]{:S(2)}) async-start(), calls=%async_computation.13 | async-start | bytes 4718592 | tf_op jit(solution)/shard_map/all_gather | solution.py:49
  447.6 157.0 %reduce-scatter.7.cloned.1.call-start = ((), (), s32[]{:S(2)}) async-start(), calls=%async_computation.7 | async-start | bytes 1572864 | tf_op jit(solution)/shard_map/reduce_scatter | solution.py:54
Sparse Core Ops, SparseCore 0:
  9.5 11.7 all-gather.6
  27.6 33.0 reduce-scatter.4
  62.3 9.0 all-gather.10
  73.4 34.2 all-gather.8
  109.6 33.0 all-gather.14
  146.8 147.8 reduce-scatter.8
  298.9 146.5 reduce-scatter.10
  448.1 73.7 all-gather.12
  524.0 70.9 all-gather.16
  597.7 6.8 reduce-scatter.6
where the time goes:
time: 612 us; the launch traced here: 611 us
  waiting for transfers between devices  540 us (88%)
  matrix products  26.8 us (4%)
  other arithmetic  20.9 us (3%)
  between operations  14.2 us (2%)
  local copies, waits for them, and re-layouts  9.29 us (2%)
    reduce_scatter x1, waiting for transfers between devices, per_device(): lax.psum_scatter(down_part, 'rep', scatter_dimension=0, tiled=True)  149 us
    reduce_scatter x1, waiting for transfers between devices, per_device(): lax.psum_scatter(up_part, 'rep', scatter_dimension=0, tiled=True)  144 us
    all_gather x1, waiting for transfers between devices, per_device(): lax.all_gather(up_slice.astype(jnp.bfloat16), 'rep', axis=0, tiled=True)  68.4 us
    all_gather x1, waiting for transfers between devices, per_device(): lax.all_gather(down_slice.astype(jnp.bfloat16), 'rep', axis=0, tiled=True)  57.1 us
    all_gather x1, waiting for transfers between devices, per_device(): lax.all_gather(grad_pre, 'fs', axis=0, tiled=True)  36.3 us
    reduce_scatter x1, waiting for transfers between devices, per_device(): lax.psum_scatter(contract_cols(rows_block, down_weight).astype(jnp.bfloat...  32.5 us
    all_gather x1, waiting for transfers between devices, per_device(): lax.all_gather(square, 'fs', axis=0, tiled=True)  27.4 us
    dot_general x2, matrix products, contract_rows(): lax.dot_general(left, right, (((0,), (0,)), ((), ())), preferred_element_...  15 us
  transfers between devices with their start and end apart: 10, of which 10 were waited for; matrix products, arithmetic and copies ran while one was open for 8% of the time, Pallas kernels for 0%

commit v1 on v0

--- a/solution.py
+++ b/solution.py
@@ -2,6 +2,7 @@
 import jax.numpy as jnp
 from jax import lax
 from jax.sharding import PartitionSpec as P
+from jax.lax import all_to_all, axis_size
 
 
 def contract_rows(left, right):
@@ -32,8 +33,17 @@
     ).astype(jnp.float32)
     grad_pre = (2.0 * positive * grad_act).astype(jnp.bfloat16)
     factor = (inputs.shape[0] * lax.axis_size("rep") * lax.axis_size("tp")) ** (-0.5)
+
+    def _replace_vectors(matrix, d0):
+        found = []
+        for _ in range(axis_size("fs")):
+            found.append(matrix)
+        view_out = all_to_all(jnp.stack(found), "fs", 0, 0)
+        v_next = jnp.concatenate(view_out, axis=d0)
+        return v_next
+
     group_grad, group_square = (
-        lax.all_gather(grad_pre, "fs", axis=0, tiled=True),
+        _replace_vectors(grad_pre, 0),
         lax.all_gather(square, "fs", axis=0, tiled=True),
     )
     down_part = contract_rows(group_square, group_cot)

time: 612 us -> 585 us (0.956)
  waiting for transfers between devices: 540 us -> 509 us
    all_gather x1 -> x0, waiting for transfers between devices: 36.3 us -> none  [per_device(): lax.all_gather(grad_pre, 'fs', axis=0, tiled=True)]
    all_to_all x0 -> x1, waiting for transfers between devices: none -> 32.5 us  [_replace_vectors(): view_out = all_to_all(jnp.stack(found), 'fs', 0, 0)]
    all_gather x1, waiting for transfers between devices: 27.4 us -> 5.54 us  [per_device(): lax.all_gather(square, 'fs', axis=0, tiled=True)]
  transfers between devices with their start and end apart: 10 -> 10, of which waited for: 10 -> 10; matrix products, arithmetic and copies ran while one was open for 8% -> 9% of each run, Pallas kernels for 0% -> 0%
where the time goes in v1:
time: 585 us
  waiting for transfers between devices  509 us (87%)
  matrix products  26.2 us (4%)
  other arithmetic  22 us (4%)
  between operations  13.9 us (2%)
  local copies, waits for them, and re-layouts  9.29 us (2%)
    reduce_scatter x1, waiting for transfers between devices, per_device(): lax.psum_scatter(down_part, 'rep', scatter_dimension=0, tiled=True)  149 us
    reduce_scatter x1, waiting for transfers between devices, per_device(): lax.psum_scatter(up_part, 'rep', scatter_dimension=0, tiled=True)  144 us
    all_gather x1, waiting for transfers between devices, per_device(): lax.all_gather(up_slice.astype(jnp.bfloat16), 'rep', axis=0, tiled=True)  68.4 us
    all_gather x1, waiting for transfers between devices, per_device(): lax.all_gather(down_slice.astype(jnp.bfloat16), 'rep', axis=0, tiled=True)  57.1 us
    all_to_all x1, waiting for transfers between devices, _replace_vectors(): view_out = all_to_all(jnp.stack(found), 'fs', 0, 0)  32.5 us
    reduce_scatter x1, waiting for transfers between devices, per_device(): lax.psum_scatter(contract_cols(rows_block, down_weight).astype(jnp.bfloat...  32.5 us
    dot_general x2, matrix products, contract_rows(): lax.dot_general(left, right, (((0,), (0,)), ((), ())), preferred_element_...  14.4 us
    mul x2, other arithmetic, per_device(): return (grad_inputs, grad_up * factor, grad_down * factor)  13.6 us
  transfers between devices with their start and end apart: 10, of which 10 were waited for; matrix products, arithmetic and copies ran while one was open for 9% of the time, Pallas kernels for 0%

profile of v1, /device:TPU:0, one launch (start us, length us, event | category | flops | bytes accessed | tf_op | source)
XLA Modules:
  0.0 584.9 jit_solution(8338524820825390034)
XLA Ops:
  7.2 0.0 all-gather.6.cloned.1.call-start
  7.2 0.7 all-gather.6.cloned.1.call-update
  7.9 0.0 copy-start
  7.9 0.0 reduce-scatter.5.cloned.1.call-start
  8.0 13.3 %all-gather.6.cloned.1.call-done = bf16[512,1024]{1,0:T(8,128)(2,1)} async-done(((bf16[256,1024]{1,0:T(8,128)(2,1)}), bf16[512,1024]{1,0:T(8,128)(2,1)}) %all-gather.6.cloned.1.call-update) | async-done | bytes 1048592 | tf_op jit(solution)/shard_map/all_gather | solution.py:23
  21.3 6.2 %convolution_convert_fusion = bf16[512,2048]{1,0:T(8,128)(2,1)} fusion(bf16[512,1024]{1,0:T(8,128)(2,1)} %all-gather.6.cloned.1.call-done, bf16[2048,1024]{1,0:T(8,128)(2,1)} %param.9), kind=kOutput, calls=%fused_computation.3 | convolution fusion | flops 2148532224 | bytes 7340032 | tf_op jit(solution)/shard_map/dot_general | solution.py:15
  27.5 0.0 reduce-scatter.5.cloned.1.call-update
  27.5 0.0 all-gather.8.cloned.1.call-start
  27.6 0.7 all-gather.8.cloned.1.call-update
  28.3 0.0 all-gather.12.cloned.1.call-start
  28.3 32.5 %reduce-scatter.5.cloned.1.call-done = bf16[256,2048]{1,0:T(8,128)(2,1)} async-done(((bf16[512,2048]{1,0:T(8,128)(2,1)}), bf16[256,2048]{1,0:T(8,128)(2,1)}) %reduce-scatter.5.cloned.1.call-update) | async-done | bytes 1048592 | tf_op jit(solution)/shard_map/reduce_scatter | solution.py:28
  60.8 0.0 copy-done
  60.8 2.8 multiply_convert_fusion
  63.5 0.0 all-gather.12.cloned.1.call-update
  63.6 1.5 pad_maximum_fusion
  65.1 3.8 all-to-all-start
  68.9 0.0 reduce-scatter.9.cloned.1.call-start
  68.9 2.5 all-gather.8.cloned.1.call-done
  71.4 32.5 %all-to-all-done = bf16[2,256,2048]{2,1,0:T(8,128)(2,1)S(1)} async-done(((bf16[2,256,2048]{2,1,0:T(8,128)(2,1)}), bf16[2,256,2048]{2,1,0:T(8,128)(2,1)S(1)}, u32[]{:S(2)}, u32[]{:S(2)}) %all-to-all-start) | async-done | bytes 2097184 | tf_op jit(solution)/shard_map/all_to_all | solution.py:41
  103.8 7.0 %convolution_bitcast_fusion = f32[1024,2048]{0,1:T(8,128)} fusion(bf16[512,2048]{1,0:T(8,128)(2,1)S(1)} %bitcast.13, bf16[512,1024]{1,0:T(8,128)(2,1)} %all-gather.8.cloned.1.call-done), kind=kOutput, calls=%fused_computation.2 | convolution fusion | flops 2147483648 | bytes 11534336 | tf_op jit(solution)/shard_map/dot_general | solution.py:9
  110.9 0.0 copy-start.1
  110.9 0.0 reduce-scatter.9.cloned.1.call-update
  110.9 0.0 reduce-scatter.11.cloned.1.call-start
  110.9 5.5 all-gather.12.cloned.1.call-done
  116.5 0.0 copy-done.1
  116.5 7.4 %fusion.1 = f32[2048,1024]{1,0:T(8,128)} fusion(bf16[512,2048]{1,0:T(8,128)(2,1)} %all-gather.12.cloned.1.call-done, bf16[512,1024]{1,0:T(8,128)(2,1)S(1)} %copy-done.1), kind=kOutput, calls=%fused_computation.10 | convolution fusion | flops 2147483648 | bytes 11534336 | tf_op jit(solution)/shard_map/dot_general | solution.py:9
  123.8 0.0 reduce-scatter.11.cloned.1.call-update
  123.9 0.0 all-gather.10.cloned.1.call-start
  123.9 144.5 %reduce-scatter.9.cloned.1.call-done = f32[128,2048]{0,1:T(8,128)} async-done(((f32[1024,2048]{0,1:T(8,128)}), f32[128,2048]{0,1:T(8,128)}) %reduce-scatter.9.cloned.1.call-update) | async-done | bytes 1048592 | tf_op jit(solution)/shard_map/reduce_scatter | solution.py:52
  268.4 2.1 convert_element_type.35
  270.5 0.0 all-gather.10.cloned.1.call-update
  270.5 0.0 all-gather.14.cloned.1.call-start
  270.5 148.5 %reduce-scatter.11.cloned.1.call-done = f32[256,1024]{1,0:T(8,128)} async-done(((f32[2048,1024]{1,0:T(8,128)}), f32[256,1024]{1,0:T(8,128)}) %reduce-scatter.11.cloned.1.call-update) | async-done | bytes 1048592 | tf_op jit(solution)/shard_map/reduce_scatter | solution.py:53
  419.0 2.1 convert_element_type.38
  421.1 0.0 all-gather.14.cloned.1.call-update
  421.2 0.2 reduce-scatter.7.cloned.1.call-start
  421.4 5.6 convolution_convert_fusion.1
  427.0 0.0 reduce-scatter.7.cloned.1.call-update
  427.1 68.4 %all-gather.10.cloned.1.call-done = bf16[1024,2048]{0,1:T(8,128)(2,1)} async-done(((bf16[128,2048]{0,1:T(8,128)(2,1)}), bf16[1024,2048]{0,1:T(8,128)(2,1)}) %all-gather.10.cloned.1.call-update) | async-done | bytes 4194320 | tf_op jit(solution)/shard_map/all_gather | solution.py:56
  495.5 6.8 %convert_multiply_fusion.1 = f32[1024,2048]{0,1:T(8,128)} fusion(bf16[1024,2048]{0,1:T(8,128)(2,1)} %all-gather.10.cloned.1.call-done), kind=kLoop, calls=%fused_computation.1 | loop fusion | flops 4194304 | bytes 12582912 | tf_op jit(solution)/shard_map/mul | solution.py:70
  502.2 9.3 %copy.8 = f32[1024,2048]{1,0:T(8,128)} copy(f32[1024,2048]{0,1:T(8,128)} %convert_multiply_fusion.1) | data formatting | bytes 16777216
  511.5 57.1 %all-gather.14.cloned.1.call-done = bf16[2048,1024]{1,0:T(8,128)(2,1)} async-done(((bf16[256,1024]{1,0:T(8,128)(2,1)}), bf16[2048,1024]{1,0:T(8,128)(2,1)}) %all-gather.14.cloned.1.call-update) | async-done | bytes 4194320 | tf_op jit(solution)/shard_map/all_gather | solution.py:59
  568.6 6.8 %convert_multiply_fusion = f32[2048,1024]{1,0:T(8,128)} fusion(bf16[2048,1024]{1,0:T(8,128)(2,1)} %all-gather.14.cloned.1.call-done), kind=kLoop, calls=%fused_computation | loop fusion | flops 4194304 | bytes 12582912 | tf_op jit(solution)/shard_map/mul | solution.py:70
  575.4 3.0 reduce-scatter.7.cloned.1.call-done
Async XLA Ops:
  7.2 14.1 %all-gather.6.cloned.1.call-start = ((), (), s32[]{:S(2)}) async-start(), calls=%async_computation.5 | async-start | bytes 1572864 | tf_op jit(solution)/shard_map/all_gather | solution.py:23
  7.9 52.9 %copy-start = (bf16[256,2048]{1,0:T(8,128)(2,1)S(1)}, bf16[256,2048]{1,0:T(8,128)(2,1)}, u32[]{:S(2)}) copy-start(bf16[256,2048]{1,0:T(8,128)(2,1)} %param.6) | copy-start | bytes 3145732
  7.9 52.9 %reduce-scatter.5.cloned.1.call-start = ((), (), s32[]{:S(2)}) async-start(), calls=%async_computation.6 | async-start | bytes 3145728 | tf_op jit(solution)/shard_map/reduce_scatter | solution.py:28
  27.5 43.9 %all-gather.8.cloned.1.call-start = ((), (), s32[]{:S(2)}) async-start(), calls=%async_computation.8 | async-start | bytes 1572864 | tf_op jit(solution)/shard_map/all_gather | solution.py:22
  28.3 88.2 %all-gather.12.cloned.1.call-start = ((), (), s32[]{:S(2)}) async-start(), calls=%async_computation.11 | async-start | bytes 3145728 | tf_op jit(solution)/shard_map/all_gather | solution.py:47
  65.1 38.8 %all-to-all-start = ((bf16[2,256,2048]{2,1,0:T(8,128)(2,1)}), bf16[2,256,2048]{2,1,0:T(8,128)(2,1)S(1)}, u32[]{:S(2)}, u32[]{:S(2)}) async-start(bf16[2,256,2048]{2,1,0:T(8,128)(2,1)} %pad_maximum_fusion), calls=%async_computation.1 | async-start | bytes 4194304 | tf_op jit(solution)/shard_map/all_to_all | solution.py:41
  68.9 199.5 %reduce-scatter.9.cloned.1.call-start = ((), (), s32[]{:S(2)}) async-start(), calls=%async_computation.9 | async-start | bytes 9437184 | tf_op jit(solution)/shard_map/reduce_scatter | solution.py:52
  110.9 5.6 copy-start.1
  110.9 308.2 %reduce-scatter.11.cloned.1.call-start = ((), (), s32[]{:S(2)}) async-start(), calls=%async_computation.12 | async-start | bytes 9437184 | tf_op jit(solution)/shard_map/reduce_scatter | solution.py:53
  123.9 371.6 %all-gather.10.cloned.1.call-start = ((), (), s32[]{:S(2)}) async-start(), calls=%async_computation.10 | async-start | bytes 4718592 | tf_op jit(solution)/shard_map/all_gather | solution.py:56
  270.5 298.1 %all-gather.14.cloned.1.call-start = ((), (), s32[]{:S(2)}) async-start(), calls=%async_computation.13 | async-start | bytes 4718592 | tf_op jit(solution)/shard_map/all_gather | solution.py:59
  421.2 157.2 %reduce-scatter.7.cloned.1.call-start = ((), (), s32[]{:S(2)}) async-start(), calls=%async_computation.7 | async-start | bytes 1572864 | tf_op jit(solution)/shard_map/reduce_scatter | solution.py:64
Sparse Core Ops, SparseCore 0:
  9.5 11.7 all-gather.5
  27.6 33.0 reduce-scatter.4
  62.3 9.0 all-gather.7
  73.4 43.0 all-gather.11
  120.5 147.8 reduce-scatter.8
  272.4 146.5 reduce-scatter.10
  421.7 73.7 all-gather.9
  497.6 70.9 all-gather.13
  571.4 6.8 reduce-scatter.6
